TPU v7x, 256 devices: a whole 4x4x8 slice. The times are simulated.
256 devices in a mesh: gr: 2 (over z_hi), fs: 16 (over z_lo, y), tp: 8 (over x, core).
Axes of the slice: x: 4, y: 4, z: 8 (z_hi: 2, z_lo: 4; z = z_hi * 4 + z_lo), core: 2. Of those that a mesh axis runs over, the one named last changes fastest.
Arguments:
- prompt: bfloat16 [24576, 2048], P(('gr', 'fs', 'tp')), may hold values from -6 to 6
- norm_first: float32 [2048], P(('gr', 'fs')), may hold values from 0.1 to 1.9
- gate_first: float32 [2048, 5632], P(('gr', 'fs'), 'tp'), may hold values from -6 to 6
- up_first: float32 [2048, 5632], P(('gr', 'fs'), 'tp'), may hold values from -6 to 6
- down_first: float32 [2048, 5632], P(('gr', 'fs'), 'tp'), may hold values from -6 to 6
- norm_second: float32 [2048], P(('gr', 'fs')), may hold values from 0.1 to 1.9
- gate_second: float32 [2048, 5632], P(('gr', 'fs'), 'tp'), may hold values from -6 to 6
- up_second: float32 [2048, 5632], P(('gr', 'fs'), 'tp'), may hold values from -6 to 6
- down_second: float32 [2048, 5632], P(('gr', 'fs'), 'tp'), may hold values from -6 to 6
Outputs:
- served_gate_first: bfloat16 [2048, 5632], P(None, 'fs')
- served_up_first: bfloat16 [2048, 5632], P(None, 'fs')
- served_down_first: bfloat16 [2048, 5632], P(None, 'fs')
- served_gate_second: bfloat16 [2048, 5632], P(None, 'fs')
- served_up_second: bfloat16 [2048, 5632], P(None, 'fs')
- served_down_second: bfloat16 [2048, 5632], P(None, 'fs')
- result: bfloat16 [24576, 2048], P(('gr', 'fs', 'tp'))
All inputs are finite; a program needn't handle non-finite values.
Results may differ from a plain program's by a relative error of at most 0.015.
Values may be sent and summed in bfloat16 or wider, within the bound.
A program may use at most 128 MiB of HBM per device.

v0:
```python
import jax
import jax.numpy as jnp
from jax import lax
from jax.sharding import Mesh
from jax.sharding import PartitionSpec as P

D = 2048
FF = 5632
FS = ("fs_0", "fs_1")
GR_FS_TP = ("gr", "fs_0", "fs_1", "tp")
GR_FS = ("gr", "fs_0", "fs_1")


EPS = 1e-06


def in_order(pieces, dim):
    dims = list(pieces.shape[1:])
    dims[dim] *= pieces.shape[0]
    return jnp.moveaxis(pieces, 0, dim).reshape(dims)


def gather_in_order(value, axes, sequence):
    pieces = value
    for k in sequence:
        pieces = lax.all_gather(pieces, axes[k])
    done = sequence[::-1]
    back = [done.index(k) for k in range(len(axes))]
    pieces = pieces.transpose(*back, *range(len(axes), pieces.ndim))
    return pieces.reshape(-1, *value.shape)


def gather_axes(value, axes, sequence, dim):
    return in_order(gather_in_order(value, axes, sequence), dim)


def fold_rows(gain, weight):
    return (gain[:, None] * weight).astype(jnp.bfloat16)


def relayout(stacked):
    moved = lax.all_to_all(
        lax.all_to_all(stacked, "tp", split_axis=1, concat_axis=2, tiled=True),
        FS,
        split_axis=2,
        concat_axis=1,
        tiled=True,
    )
    whole = lax.all_gather(moved, ("gr", "tp"), axis=1, tiled=True)
    matrices = stacked.shape[0]
    block_width = moved.shape[2]
    gr_size = lax.axis_size("gr")
    tp_size = lax.axis_size("tp")
    fs_size = lax.axis_size(FS)
    sub_rows = stacked.shape[1] // tp_size
    shaped = whole.reshape(matrices, gr_size, tp_size, fs_size, sub_rows, block_width)
    return shaped.transpose(0, 1, 3, 2, 4, 5).reshape(
        matrices, gr_size * fs_size * tp_size * sub_rows, block_width
    )


def half_step(residual, weights):
    gate_weight = weights[0]
    up_weight = weights[1]
    down_weight = weights[2]
    resid_f = residual.astype(jnp.float32)
    normed = (
        resid_f * lax.rsqrt(jnp.mean(resid_f * resid_f, axis=-1, keepdims=True) + EPS)
    ).astype(jnp.bfloat16)
    in_scale = D ** (-0.5)
    out_scale = FF ** (-0.5)
    tokens_in = gather_axes(normed, FS, (0, 1), 0)
    gate_pre = jnp.dot(tokens_in, gate_weight, preferred_element_type=jnp.float32) * in_scale
    up_pre = jnp.dot(tokens_in, up_weight, preferred_element_type=jnp.float32) * in_scale
    hidden = (jax.nn.silu(gate_pre) * up_pre).astype(jnp.bfloat16)
    branch = lax.psum_scatter(
        (
            lax.dot_general(
                hidden, down_weight, (((1,), (1,)), ((), ())), preferred_element_type=jnp.float32
            )
            * out_scale
        ).astype(jnp.bfloat16),
        FS,
        scatter_dimension=0,
        tiled=True,
    ).astype(jnp.float32)
    return (resid_f + 0.5 * branch).astype(jnp.bfloat16)


def on_device(
    prompt,
    norm_first,
    gate_first,
    up_first,
    down_first,
    norm_second,
    gate_second,
    up_second,
    down_second,
):
    first_set = jnp.stack(
        [
            fold_rows(norm_first, gate_first),
            fold_rows(norm_first, up_first),
            down_first.astype(jnp.bfloat16),
        ]
    )
    second_set = jnp.stack(
        [
            fold_rows(norm_second, gate_second),
            fold_rows(norm_second, up_second),
            down_second.astype(jnp.bfloat16),
        ]
    )
    joined = relayout(jnp.concatenate([first_set, second_set], axis=0))
    served_first = joined[:3]
    served_second = joined[3:]
    middle = half_step(prompt, served_first)
    result = half_step(middle, served_second)
    return (
        served_first[0],
        served_first[1],
        served_first[2],
        served_second[0],
        served_second[1],
        served_second[2],
        result,
    )


def solution(mesh):
    split = Mesh(
        mesh.devices.reshape(mesh.shape["gr"], 4, 4, mesh.shape["tp"]), ("gr", "fs_0", "fs_1", "tp")
    )
    in_specs = (
        P(GR_FS_TP, None),
        P(GR_FS),
        P(GR_FS, "tp"),
        P(GR_FS, "tp"),
        P(GR_FS, "tp"),
        P(GR_FS),
        P(GR_FS, "tp"),
        P(GR_FS, "tp"),
        P(GR_FS, "tp"),
    )
    out_specs = (
        P(None, FS),
        P(None, FS),
        P(None, FS),
        P(None, FS),
        P(None, FS),
        P(None, FS),
        P(GR_FS_TP, None),
    )
    return jax.shard_map(
        on_device, mesh=split, in_specs=in_specs, out_specs=out_specs, check_vma=False
    )
```

profile of v0, /device:TPU:2, one launch (start us, length us, event | category | flops | bytes accessed | tf_op | source)
XLA Modules:
  0.0 613.4 jit_solution(5600202957477131407)
XLA Ops:
  7.2 0.0 all-gather.12.cloned.1.call-start
  7.3 1.3 fusion.4
  8.6 0.0 copy-start.16
  8.6 1.9 fusion.5
  10.6 0.0 all-gather.12.cloned.1.call-update
  10.6 0.0 all-gather.14.cloned.1.call-start
  10.6 44.8 %all-gather.12.cloned.1.call-done = bf16[384,2048]{1,0:T(8,128)(2,1)} async-done(((bf16[96,2048]{1,0:T(8,128)(2,1)}), bf16[384,2048]{1,0:T(8,128)(2,1)}) %all-gather.12.cloned.1.call-update) | async-done | bytes 1572880 | tf_op jit(solution)/shard_map/all_gather | solution.py:26
  55.4 0.0 all-gather.14.cloned.1.call-update
  55.5 0.0 all-gather.10.cloned.1.call-start
  55.5 0.1 fusion.11
  55.6 0.0 copy-done.12
  55.6 0.1 fusion.13
  55.7 0.0 copy-done.18
  55.7 0.0 copy-done.14
  55.8 0.1 fusion.15
  55.9 0.1 fusion.17
  56.0 0.3 copy.65
  56.3 16.4 %all_to_all.36 = bf16[6,64,704]{2,0,1:T(8,128)(2,1)S(1)} all-to-all(bf16[6,64,704]{2,0,1:T(8,128)(2,1)S(1)} %copy.65), channel_id=1, replica_groups=mesh['gr'=2,'fs_0'=4,'fs_1'=4,'tp'=8] {'tp'}, dimensions={1} | all-to-all | bytes 1081344 | tf_op jit(solution)/shard_map/all_to_all | solution.py:43
  72.7 8.9 %copy.83 = bf16[6,8,8,704]{1,0,3,2:T(8,128)(2,1)} copy(bf16[6,8,8,704]{3,0,1,2:T(8,128)(2,1)S(1)} %bitcast.81) | data formatting | bytes 1081344 | tf_op jit(solution)/shard_map/all_to_all | solution.py:43
  81.5 11.3 %reshape.55 = bf16[16,2,8448]{2,1,0:T(2,128)(2,1)S(1)} reshape(bf16[5632,6,8]{2,1,0:T(8,128)(2,1)} %bitcast.60) | data formatting | bytes 1081344
  92.8 21.6 %all_to_all.37 = bf16[16,2,8448]{2,1,0:T(2,128)(2,1)S(1)} all-to-all(bf16[16,2,8448]{2,1,0:T(2,128)(2,1)S(1)} %reshape.55), channel_id=1, replica_groups=mesh['gr'=2,'fs_0'=4,'fs_1'=4,'tp'=8] {'fs_0','fs_1'}, dimensions={0} | all-to-all | bytes 1081344 | tf_op jit(solution)/shard_map/all_to_all | solution.py:42
  114.4 11.8 %reshape.56 = bf16[5632,6,8]{2,1,0:T(8,128)(2,1)} reshape(bf16[16,2,8448]{2,1,0:T(2,128)(2,1)S(1)} %all_to_all.37) | data formatting | bytes 1081344
  126.3 9.7 %copy.68 = bf16[6,8,16,352]{3,1,2,0:T(8,128)(2,1)} copy(bf16[6,8,16,352]{1,0,3,2:T(8,128)(2,1)} %bitcast.61) | data formatting | bytes 1081344 | tf_op jit(solution)/shard_map/all_to_all | solution.py:42
  136.0 0.0 all-gather.10.cloned.1.call-update
  136.0 0.2 reduce-scatter.3.cloned.1.call-start
  136.3 0.0 all-gather.14.cloned.1.call-done
  136.3 6.6 %copy.75 = bf16[4,4,96,2048]{3,2,1,0:T(8,128)(2,1)} copy(bf16[4,4,96,2048]{3,2,0,1:T(8,128)(2,1)} %bitcast.63) | data formatting | bytes 12582912 | tf_op jit(solution)/shard_map/transpose | solution.py:29
  142.9 106.5 %all-gather.10.cloned.1.call-done = bf16[6,2048,352]{2,1,0:T(8,128)(2,1)} async-done(((bf16[6,128,352]{2,1,0:T(8,128)(2,1)}), bf16[6,2048,352]{2,1,0:T(8,128)(2,1)}) %all-gather.10.cloned.1.call-update) | async-done | bytes 8650768 | tf_op jit(solution)/shard_map/all_gather | solution.py:49
  249.4 6.1 fusion.22
  255.4 0.3 copy.69
  255.7 0.3 copy.70
  256.0 1.4 copy.71
  257.4 1.7 copy-done.1
  259.1 3.9 convolution_multiply_fusion.3
  263.0 12.0 %multiply_convert_fusion.1 = bf16[1536,2048]{1,0:T(8,128)(2,1)} fusion(bf16[2048,352]{1,0:T(8,128)(2,1)} %bitcast.73, bf16[1536,2048]{1,0:T(8,128)(2,1)} %bitcast.64, bf16[2048,352]{1,0:T(8,128)(2,1)S(1)} %bitcast.71, f32[1536,352]{0,1:T(8,128)} %convolution_multiply_fusion.3), kind=kOutput, calls=%fused_computation.1 | convolution fusion | flops 4439261184 | bytes 17629184 | tf_op jit(solution)/shard_map/dot_general | solution.py:78
  275.0 0.0 reduce-scatter.3.cloned.1.call-update
  275.0 0.0 all-gather.16.cloned.1.call-start
  275.1 96.4 %reduce-scatter.3.cloned.1.call-done = bf16[96,2048]{1,0:T(8,128)(2,1)} async-done(((bf16[1536,2048]{1,0:T(8,128)(2,1)}), bf16[96,2048]{1,0:T(8,128)(2,1)}) %reduce-scatter.3.cloned.1.call-update) | async-done | bytes 393232 | tf_op jit(solution)/shard_map/reduce_scatter | solution.py:76
  371.5 1.2 fusion.7
  372.8 1.9 fusion.8
  374.7 0.0 all-gather.16.cloned.1.call-update
  374.7 0.0 all-gather.18.cloned.1.call-start
  374.7 38.8 %all-gather.16.cloned.1.call-done = bf16[384,2048]{1,0:T(8,128)(2,1)} async-done(((bf16[96,2048]{1,0:T(8,128)(2,1)}), bf16[384,2048]{1,0:T(8,128)(2,1)}) %all-gather.16.cloned.1.call-update) | async-done | bytes 1572880 | tf_op jit(solution)/shard_map/all_gather | solution.py:26
  413.5 0.0 all-gather.18.cloned.1.call-update
  413.5 0.3 reduce-scatter.5.cloned.1.call-start
  413.8 2.9 copy.72
  416.8 0.0 copy-done.5
  416.8 1.4 copy.73
  418.2 0.4 copy-done.4
  418.6 1.5 copy.74
  420.0 62.7 %all-gather.18.cloned.1.call-done = bf16[16,96,2048]{2,1,0:T(8,128)(2,1)} async-done(((bf16[4,96,2048]{2,1,0:T(8,128)(2,1)}), bf16[16,96,2048]{2,1,0:T(8,128)(2,1)}) %all-gather.18.cloned.1.call-update) | async-done | bytes 6291472 | tf_op jit(solution)/shard_map/all_gather | solution.py:26
  482.7 3.5 copy.76
  486.2 3.8 convolution_multiply_fusion.1
  490.1 12.5 %multiply_convert_fusion = bf16[1536,2048]{1,0:T(8,128)(2,1)} fusion(bf16[2048,352]{1,0:T(8,128)(2,1)} %bitcast.79, bf16[1536,2048]{1,0:T(8,128)(2,1)} %bitcast.68, bf16[2048,352]{1,0:T(8,128)(2,1)} %bitcast.77, f32[1536,352]{0,1:T(8,128)} %convolution_multiply_fusion.1), kind=kOutput, calls=%fused_computation | convolution fusion | flops 4439261184 | bytes 17629184 | tf_op jit(solution)/shard_map/dot_general | solution.py:78
  502.6 0.0 reduce-scatter.5.cloned.1.call-update
  502.6 1.6 copy.77
  504.2 1.6 copy.78
  505.7 1.6 copy.79
  507.3 1.6 copy.80
  508.9 0.0 copy-done.8
  508.9 1.6 copy.81
  510.5 1.6 copy.82
  512.1 92.5 %reduce-scatter.5.cloned.1.call-done = bf16[96,2048]{1,0:T(8,128)(2,1)} async-done(((bf16[1536,2048]{1,0:T(8,128)(2,1)}), bf16[96,2048]{1,0:T(8,128)(2,1)}) %reduce-scatter.5.cloned.1.call-update) | async-done | bytes 393232 | tf_op jit(solution)/shard_map/reduce_scatter | solution.py:76
  604.6 1.9 fusion.9
  (34 shorter events, 0.1 us)
Async XLA Ops:
  7.2 48.3 %copy-start.17 = (f32[64]{0:T(128)S(1)}, f32[64]{0:T(128)}, u32[]{:S(2)}) copy-start(f32[64]{0:T(128)} %param.10) | copy-start | bytes 772
  7.2 48.3 %copy-start.11 = (f32[64,704]{1,0:T(8,128)S(1)}, f32[64,704]{1,0:T(8,128)}, u32[]{:S(2)}) copy-start(f32[64,704]{1,0:T(8,128)} %param.11) | copy-start | bytes 540676
  7.2 48.4 %copy-start.12 = (f32[64,704]{1,0:T(8,128)S(1)}, f32[64,704]{1,0:T(8,128)}, u32[]{:S(2)}) copy-start(f32[64,704]{1,0:T(8,128)} %param.12) | copy-start | bytes 540676
  7.2 48.5 %copy-start.13 = (f32[64,704]{1,0:T(8,128)S(1)}, f32[64,704]{1,0:T(8,128)}, u32[]{:S(2)}) copy-start(f32[64,704]{1,0:T(8,128)} %param.13) | copy-start | bytes 540676
  7.2 48.5 %copy-start.18 = (f32[64]{0:T(128)S(1)}, f32[64]{0:T(128)}, u32[]{:S(2)}) copy-start(f32[64]{0:T(128)} %param.14) | copy-start | bytes 772
  7.2 48.5 %copy-start.14 = (f32[64,704]{1,0:T(8,128)S(1)}, f32[64,704]{1,0:T(8,128)}, u32[]{:S(2)}) copy-start(f32[64,704]{1,0:T(8,128)} %param.15) | copy-start | bytes 540676
  7.2 48.6 %copy-start.15 = (f32[64,704]{1,0:T(8,128)S(1)}, f32[64,704]{1,0:T(8,128)}, u32[]{:S(2)}) copy-start(f32[64,704]{1,0:T(8,128)} %param.16) | copy-start | bytes 540676
  7.2 48.2 %all-gather.12.cloned.1.call-start = ((), (), s32[]{:S(2)}) async-start(), calls=%async_computation.7 | async-start | bytes 1966080 | tf_op jit(solution)/shard_map/all_gather | solution.py:26
  8.6 47.3 %copy-start.16 = (f32[64,704]{1,0:T(8,128)S(1)}, f32[64,704]{1,0:T(8,128)}, u32[]{:S(2)}) copy-start(f32[64,704]{1,0:T(8,128)} %param.17) | copy-start | bytes 540676
  10.6 125.7 %all-gather.14.cloned.1.call-start = ((), (), s32[]{:S(2)}) async-start(), calls=%async_computation.8 | async-start | bytes 7864320 | tf_op jit(solution)/shard_map/all_gather | solution.py:26
  55.5 193.9 %all-gather.10.cloned.1.call-start = ((), (), s32[]{:S(2)}) async-start(), calls=%async_computation.4 | async-start | bytes 10027008 | tf_op jit(solution)/shard_map/all_gather | solution.py:49
  136.0 235.4 %reduce-scatter.3.cloned.1.call-start = ((), (), s32[]{:S(2)}) async-start(), calls=%async_computation.5 | async-start | bytes 6684672 | tf_op jit(solution)/shard_map/reduce_scatter | solution.py:76
  255.7 3.4 copy-start.1
  275.0 96.5 %copy-start = (bf16[96,2048]{1,0:T(8,128)(2,1)S(1)}, bf16[96,2048]{1,0:T(8,128)(2,1)}, u32[]{:S(2)}) copy-start(bf16[96,2048]{1,0:T(8,128)(2,1)} %param.9) | copy-start | bytes 1179652
  275.0 138.5 %all-gather.16.cloned.1.call-start = ((), (), s32[]{:S(2)}) async-start(), calls=%async_computation.9 | async-start | bytes 1966080 | tf_op jit(solution)/shard_map/all_gather | solution.py:26
  374.7 108.0 %all-gather.18.cloned.1.call-start = ((), (), s32[]{:S(2)}) async-start(), calls=%async_computation.10 | async-start | bytes 7864320 | tf_op jit(solution)/shard_map/all_gather | solution.py:26
  413.5 191.0 %reduce-scatter.5.cloned.1.call-start = ((), (), s32[]{:S(2)}) async-start(), calls=%async_computation.6 | async-start | bytes 6684672 | tf_op jit(solution)/shard_map/reduce_scatter | solution.py:76
  413.8 3.0 copy-start.5
  416.8 1.8 copy-start.4
  482.7 3.5 copy-start.6
  486.2 3.9 copy-start.2
  504.2 1.6 copy-start.3
  505.7 1.6 copy-start.7
  507.3 1.6 copy-start.8
  508.9 1.6 copy-start.9
  510.5 94.1 %copy-start.10 = (bf16[96,2048]{1,0:T(8,128)(2,1)S(1)}, bf16[96,2048]{1,0:T(8,128)(2,1)}, u32[]{:S(2)}) copy-start(bf16[96,2048]{1,0:T(8,128)(2,1)} %reduce-scatter.3.cloned.1.call-done) | copy-start | bytes 1179652
Sparse Core Ops, SparseCore 0:
  10.7 44.6 all-gather.11
  57.2 73.2 all-gather.13
  136.2 113.1 all-gather.9
  275.1 96.2 reduce-scatter.2
  374.8 38.6 all-gather.15
  415.2 67.4 all-gather.17
  502.7 101.8 reduce-scatter.4
where the time goes:
time: 614 us; the launch traced here: 613 us
  waiting for transfers between devices  442 us (72%)
  local copies, waits for them, and re-layouts  77.5 us (13%)
  blocking collectives  38 us (6%)
  matrix products  32.3 us (5%)
  between operations  14.4 us (2%)
  other arithmetic  8.68 us (1%)
    reduce_scatter x2, waiting for transfers between devices, half_step(): lax.psum_scatter((lax.dot_general(hidden, down_weight, (((1,), (1,)), (()...  189 us
    all_gather x4, waiting for transfers between devices, gather_in_order(): pieces = lax.all_gather(pieces, axes[k])  146 us
    all_gather x1, waiting for transfers between devices, relayout(): whole = lax.all_gather(moved, ('gr', 'tp'), axis=1, tiled=True)  107 us
    unnamed x46, local copies, waits for them, and re-layouts  34.7 us
    dot_general x2, matrix products, half_step(): lax.dot_general(hidden, down_weight, (((1,), (1,)), ((), ())), preferred_...  24.5 us
    all_to_all x1, blocking collectives, relayout(): lax.all_to_all(lax.all_to_all(stacked, 'tp', split_axis=1, concat_axis=2,...  21.6 us
    all_to_all x1, blocking collectives, relayout(): lax.all_to_all(stacked, 'tp', split_axis=1, concat_axis=2, tiled=True)  16.4 us
  transfers between devices with their start and end apart: 7, of which 6 were waited for; matrix products, arithmetic and copies ran while one was open for 10% of the time, Pallas kernels for 0%

commit v1 on v0

v1 whole, which is shorter than its diff:
```python
import jax
import jax.numpy as jnp
from jax import lax
from jax.experimental import pallas as pl
from jax.experimental.pallas import tpu as pltpu
from jax.sharding import PartitionSpec as P

D = 2048
FF = 5632
EPS = 1e-06
NY, NZ, NX = 4, 8, 4
TOK = 96
HALF = 48
ROWS = 64
PIECE = 32
COLS = 704
BLK = 352
PAD = 384
PACK = 2176
GU = 1408
DN = 768
SERVED = 3 * PAD
NR = 17
LANES = ((0, 768), (768, 640), (1408, 768))
CH = 512
NCH = D // CH
IN_SCALE = D ** (-0.5)
OUT_SCALE = FF ** (-0.5)
ROUNDS = 2 * NR + 10


def kernel(
    packed,
    prompt,
    served,
    result,
    wall,
    xa,
    pre,
    hid,
    accs,
    own,
    part,
    st2,
    comb,
    cbuf,
    rbuf,
    resid,
    stage,
    load_sem,
    ring_recv,
    ring_send,
    d2d_recv,
    d2d_send,
    srecv,
    s_fwd_send,
    s_d2d_send,
    s_d2d_recv,
    ag_recv,
    ag_send,
    c_recv,
    c_send,
    r_recv,
    r_send,
):
    gr = lax.axis_index("gr")
    fs = lax.axis_index("fs")
    tp = lax.axis_index("tp")
    z_lo, y = fs // NY, fs % NY
    z = gr * 4 + z_lo
    x, core = tp // 2, tp % 2
    s = (y + z) % 4

    def dev(yy, zz, xx, cc):
        return (zz // 4, (zz % 4) * NY + yy, xx * 2 + cc)

    y_up, y_dn = (y + 1) % NY, (y + NY - 1) % NY
    z_up, z_dn = (z + 1) % NZ, (z + NZ - 1) % NZ
    last = s // 3
    first = (4 - s) // 4

    def pick(flag, a, b):
        return flag * a + (1 - flag) * b

    nbr = (
        (
            dev(pick(last, y_up, y), pick(last, z, z_up), x, core),
            dev(pick(first, y_dn, y), pick(first, z, z_dn), x, core),
        ),
        (
            dev(pick(last, y, y_up), pick(last, z_up, z), x, core),
            dev(pick(first, y, y_dn), pick(first, z_dn, z), x, core),
        ),
    )
    partner = dev(y, z, x, 1 - core)
    right = dev(y, z, (x + 1) % NX, core)
    left = dev(y, z, (x + NX - 1) % NX, core)
    x_r, x_l, x_far = (x + 1) % NX, (x + NX - 1) % NX, (x + 2) % NX

    def piece_row(h, d, k):
        if d == 0:
            t = (k - s + 3) // 4
            dy, dz = (t, k - t) if h == 0 else (k - t, t)
            yy, zz = (y - dy + 32) % NY, (z - dz + 32) % NZ
        else:
            t = (s + k) // 4
            dy, dz = (t, k - t) if h == 0 else (k - t, t)
            yy, zz = (y + dy) % NY, (z + dz) % NZ
        return pl.multiple_of((zz * NY + yy) * ROWS + h * PIECE, PIECE)

    def remote(src, dst, send, recv, device):
        return pltpu.make_async_remote_copy(
            src_ref=src,
            dst_ref=dst,
            send_sem=send,
            recv_sem=recv,
            device_id=device,
            device_id_type=pl.DeviceIdType.MESH,
        )

    def wait_for(ref, sem):
        pltpu.make_async_copy(ref, ref, sem).wait()

    my_rows = pl.ds(pl.multiple_of((z * NY + y) * ROWS, ROWS), ROWS)
    loads = [
        pltpu.make_async_copy(packed.at[t], wall.at[t, core, my_rows], load_sem.at[t])
        for t in range(2)
    ]
    for load in loads:
        load.start()

    barrier = pltpu.get_barrier_semaphore()
    everyone = (
        dev(y_up, z, x, core),
        dev(y_dn, z, x, core),
        dev(y, z_up, x, core),
        dev(y, z_dn, x, core),
        right,
        left,
        partner,
    )
    for device in everyone:
        pl.semaphore_signal(barrier, inc=1, device_id=device, device_id_type=pl.DeviceIdType.MESH)
    pl.semaphore_wait(barrier, len(everyone))
    for load in loads:
        load.wait()

    def ring_round(R):
        t = R // NR
        r = R % NR
        rows = {(h, d): pl.ds(piece_row(h, d, r), PIECE) for h in range(2) for d in range(2)}
        for m, (lane, width) in enumerate(LANES):
            for d in range(2):
                end = 16 - d
                blocks = [wall.at[t, core, rows[h, d], pl.ds(lane, width)] for h in range(2)]

                @pl.when(jnp.logical_and(r >= 1, r <= end))
                def _():
                    for h in range(2):
                        wait_for(blocks[h], ring_recv.at[R, h, d, m])

                @pl.when(r < end)
                def _():
                    for h in range(2):
                        remote(
                            blocks[h],
                            blocks[h],
                            ring_send.at[t, h, d],
                            ring_recv.at[R + 1, h, d, m],
                            nbr[h][d],
                        ).start()

        for d in range(2):

            @pl.when(jnp.logical_and(r >= d, r <= 16 - d))
            def _():
                for h in range(2):
                    block = wall.at[t, core, rows[h, d]]
                    remote(block, block, d2d_send.at[t], d2d_recv.at[t], partner).start()

    serves = core == y // 2
    dist = ((x - z_lo + NX) % NX, (z_lo - x + NX) % NX)
    side = (right, left)

    def cut(R):
        t = R // NR
        r = R % NR
        for d in range(2):

            @pl.when(jnp.logical_and(r >= d, r <= 16 - d))
            def _():
                for h in range(2):
                    row = piece_row(h, d, r)
                    for m, lane in enumerate((0, 640, 1408)):
                        window = wall[t, core, pl.ds(row, PIECE), lane : lane + 768]
                        window = window.astype(jnp.float32)
                        start = (64 if m == 1 else 0) + BLK * (y % 2)
                        block = pltpu.roll(window, (768 - start) % 768, 1)[:, :PAD]
                        stage[R % 2, h, d, :, m * PAD : (m + 1) * PAD] = block.astype(jnp.bfloat16)
                    pltpu.make_async_copy(
                        stage.at[R % 2, h, d],
                        served.at[t, pl.ds(row, PIECE)],
                        srecv.at[R, h, d],
                    ).start()

    def pass_on(R):
        for h in range(2):
            was = R - 2 * dist[h] - 1

            @pl.when(jnp.logical_and(was >= 0, was < 2 * NR))
            def _():
                t = was // NR
                r = was % NR
                for d in range(2):

                    @pl.when(jnp.logical_and(r >= d, r <= 16 - d))
                    def _():
                        block = served.at[t, pl.ds(piece_row(h, d, r), PIECE)]
                        wait_for(block, srecv.at[was, h, d])

                        @pl.when(dist[h] < 3)
                        def _():
                            remote(
                                block, block, s_fwd_send.at[h], srecv.at[was, h, d], side[h]
                            ).start()

                        remote(block, block, s_d2d_send, s_d2d_recv, partner).start()

    def normed(value):
        square = jnp.mean(value * value, axis=-1, keepdims=True)
        return (value * lax.rsqrt(square + EPS)).astype(jnp.bfloat16)

    halves = (pl.ds(0, HALF), pl.ds(HALF, HALF))

    def send_tokens(p):
        for i, device in enumerate((right, left)):
            for b in range(2):
                block = xa.at[p, x, halves[b]]
                remote(block, block, ag_send.at[p, i, b], ag_recv.at[p, i, b], device).start()

    def relay_tokens(p):
        for i, (device, origin) in enumerate(((right, x_l), (left, x_r))):
            block = xa.at[p, origin, halves[i]]
            wait_for(block, ag_recv.at[p, i, i])
            remote(block, block, ag_send.at[p, i, 2], ag_recv.at[p, i, 2], device).start()

    def await_tokens(p):
        for i, origin in enumerate((x_l, x_r)):
            wait_for(xa.at[p, origin, halves[1 - i]], ag_recv.at[p, i, 1 - i])
            wait_for(xa.at[p, x_far, halves[i]], ag_recv.at[p, i, 2])

    def hidden(t, c):
        tokens = xa[t].reshape(NX * TOK, D)
        pre[...] = jnp.dot(tokens, wall[t, c, :, :GU], preferred_element_type=jnp.float32)

        def rows_of(i, carry):
            rows = pl.ds(pl.multiple_of(i * HALF, HALF), HALF)
            gate = pre[rows, :DN] * IN_SCALE
            up = pltpu.roll(pre[rows, GU - DN :], DN - 64, 1) * IN_SCALE
            value = gate / (1.0 + jnp.exp(-gate)) * up
            lane = lax.broadcasted_iota(jnp.int32, value.shape, 1)
            hid[c, rows, :] = jnp.where(lane < COLS, value, 0.0).astype(jnp.bfloat16)
            return carry

        lax.fori_loop(0, NX * TOK // HALF, rows_of, 0)

    def down(t, j):
        drows = pl.ds(pl.multiple_of(j * CH, CH), CH)
        total = None
        for c in range(2):
            term = lax.dot_general(
                hid[c],
                wall[t, c, drows, GU:],
                (((1,), (1,)), ((), ())),
                preferred_element_type=jnp.float32,
            )
            total = term if total is None else total + term
        accs[...] = (total * OUT_SCALE).reshape(NX, TOK, CH)
        own[:, drows] = accs[x]
        part[0, :, drows] = accs[x_r]
        part[1, :, drows] = accs[x_l]
        st2[t, :, drows] = accs[x_far].astype(jnp.bfloat16)
        for i, device in enumerate((right, left)):
            remote(
                st2.at[t, halves[i], drows],
                cbuf.at[t, i, :, drows],
                c_send.at[t, i, j],
                c_recv.at[t, i, j],
                device,
            ).start()

    def combine(t, j):
        drows = pl.ds(pl.multiple_of(j * CH, CH), CH)
        for i, device in enumerate((right, left)):
            wait_for(cbuf.at[t, i, :, drows], c_recv.at[t, i, j])
            comb[t, i, halves[i], drows] = (
                part[i, halves[i], drows] + cbuf[t, i, :, drows].astype(jnp.float32)
            ).astype(jnp.bfloat16)
            comb[t, i, halves[1 - i], drows] = part[i, halves[1 - i], drows].astype(jnp.bfloat16)
            remote(
                comb.at[t, i, :, drows],
                rbuf.at[t, i, :, drows],
                r_send.at[t, i, j],
                r_recv.at[t, i, j],
                device,
            ).start()

    def finish(t):
        for j in range(NCH):
            for i in range(2):
                wait_for(rbuf.at[t, i, :, pl.ds(j * CH, CH)], r_recv.at[t, i, j])
        branch = own[...] + rbuf[t, 0].astype(jnp.float32) + rbuf[t, 1].astype(jnp.float32)
        return (resid[...] + 0.5 * branch).astype(jnp.bfloat16)

    start = prompt[...].astype(jnp.float32)
    resid[...] = start
    xa[0, x] = normed(start)

    def one_round(R, carry):
        @pl.when(R < 2 * NR)
        def _():
            ring_round(R)

        @pl.when(R == 0)
        def _():
            send_tokens(0)

        @pl.when(serves)
        def _():
            pass_on(R)

            @pl.when(jnp.logical_and(x == z_lo, R < 2 * NR))
            def _():
                cut(R)

        @pl.when(R == 3)
        def _():
            relay_tokens(0)

        @pl.when(R == NR - 1)
        def _():
            await_tokens(0)

        @pl.when(R == NR + 11)
        def _():
            relay_tokens(1)

        @pl.when(R == 2 * NR - 1)
        def _():
            await_tokens(1)

        t = (R - NR + NR) // NR - 1
        q = R % NR

        @pl.when(R >= NR)
        def _():
            @pl.when(q == 1)
            def _():
                wait_for(wall.at[t, 1 - core], d2d_recv.at[t])

            @pl.when(q < 2)
            def _():
                hidden(t, (core + q) % 2)

            @pl.when(jnp.logical_and(q >= 2, q < 2 + NCH))
            def _():
                down(t, q - 2)

            @pl.when(jnp.logical_and(q >= 4, q < 4 + NCH))
            def _():
                combine(t, q - 4)

        @pl.when(R == NR + 9)
        def _():
            middle = finish(0).astype(jnp.float32)
            resid[...] = middle
            xa[1, x] = normed(middle)
            send_tokens(1)

        @pl.when(R == 2 * NR + 9)
        def _():
            result[...] = finish(1)

        return carry

    lax.fori_loop(0, ROUNDS, one_round, 0)

    for t in range(2):
        for h in range(2):
            wait_for(wall.at[t, 0, pl.ds(0, 16 * PIECE)], ring_send.at[t, h, 0])
            wait_for(wall.at[t, 0, pl.ds(0, 15 * PIECE)], ring_send.at[t, h, 1])
        wait_for(wall.at[t, core], d2d_send.at[t])
        for i in range(2):
            for b in range(3):
                wait_for(xa.at[t, x, halves[0]], ag_send.at[t, i, b])
            for j in range(NCH):
                block = pl.ds(j * CH, CH)
                wait_for(st2.at[t, halves[i], block], c_send.at[t, i, j])
                wait_for(comb.at[t, i, :, block], r_send.at[t, i, j])

    @pl.when(serves)
    def _():
        for h in range(2):

            @pl.when(dist[h] < 3)
            def _():
                wait_for(served.at[0], s_fwd_send.at[h])

        wait_for(served, s_d2d_send)

    @pl.when(jnp.logical_not(serves))
    def _():
        wait_for(served, s_d2d_recv)


def on_device(
    prompt,
    norm_first,
    gate_first,
    up_first,
    down_first,
    norm_second,
    gate_second,
    up_second,
    down_second,
):
    def pack(gain, gate, up, down):
        gain = gain[:, None]
        zero = jnp.zeros((ROWS, PACK - 3 * COLS), jnp.float32)
        return jnp.concatenate([gain * gate, gain * up, down, zero], axis=1).astype(jnp.bfloat16)

    packed = jnp.stack(
        [
            pack(norm_first, gate_first, up_first, down_first),
            pack(norm_second, gate_second, up_second, down_second),
        ]
    )
    dma = pltpu.SemaphoreType.DMA
    bf16, f32 = jnp.bfloat16, jnp.float32
    served, result = pl.pallas_call(
        kernel,
        out_shape=(
            jax.ShapeDtypeStruct((2, D, SERVED), bf16),
            jax.ShapeDtypeStruct((TOK, D), bf16),
        ),
        in_specs=[
            pl.BlockSpec(memory_space=pl.ANY),
            pl.BlockSpec(memory_space=pltpu.VMEM),
        ],
        out_specs=(
            pl.BlockSpec(memory_space=pl.ANY),
            pl.BlockSpec(memory_space=pltpu.VMEM),
        ),
        scratch_shapes=[
            pltpu.VMEM((2, 2, D, PACK), bf16),
            pltpu.VMEM((2, NX, TOK, D), bf16),
            pltpu.VMEM((NX * TOK, GU), f32),
            pltpu.VMEM((2, NX * TOK, DN), bf16),
            pltpu.VMEM((NX, TOK, CH), f32),
            pltpu.VMEM((TOK, D), f32),
            pltpu.VMEM((2, TOK, D), f32),
            pltpu.VMEM((2, TOK, D), bf16),
            pltpu.VMEM((2, 2, TOK, D), bf16),
            pltpu.VMEM((2, 2, HALF, D), bf16),
            pltpu.VMEM((2, 2, TOK, D), bf16),
            pltpu.VMEM((TOK, D), f32),
            pltpu.VMEM((2, 2, 2, PIECE, SERVED), bf16),
            dma((2,)),
            dma((2 * NR, 2, 2, 3)),
            dma((2, 2, 2)),
            dma((2,)),
            dma((2,)),
            dma((2 * NR, 2, 2)),
            dma((2,)),
            dma,
            dma,
            dma((2, 2, 3)),
            dma((2, 2, 3)),
            dma((2, 2, NCH)),
            dma((2, 2, NCH)),
            dma((2, 2, NCH)),
            dma((2, 2, NCH)),
        ],
        compiler_params=pltpu.CompilerParams(
            collective_id=0, has_side_effects=True, vmem_limit_bytes=66 * 1024 * 1000
        ),
    )(packed, prompt)
    blocks = [served[t, :, m * PAD : m * PAD + BLK] for t in range(2) for m in range(3)]
    return (*blocks, result)


def solution(mesh):
    row = P(("gr", "fs"))
    tile = P(("gr", "fs"), "tp")
    token = P(("gr", "fs", "tp"), None)
    block = P(None, "fs")
    return jax.shard_map(
        on_device,
        mesh=mesh,
        in_specs=(token, row, tile, tile, tile, row, tile, tile, tile),
        out_specs=(block,) * 6 + (token,),
        check_vma=False,
    )
```

time: 614 us -> 194 us (0.32)
  waiting for transfers between devices: 442 us -> 0 us
  Pallas kernels: 0 us -> 169 us
  local copies, waits for them, and re-layouts: 77.5 us -> 21.1 us
  blocking collectives: 38 us -> 0 us
  matrix products: 32.3 us -> 0 us
  between operations: 14.4 us -> 0.73 us
    all_gather x5 -> x0, waiting for transfers between devices: 253 us -> none  [the longest x4 146 us: gather_in_order(): pieces = lax.all_gather(pieces, axes[k])]
    reduce_scatter x2 -> x0, waiting for transfers between devices: 189 us -> none  [half_step(): lax.psum_scatter((lax.dot_general(hidden, down_weight, (((1,), (1,)), (()...]
    pallas_call x0 -> x1, Pallas kernels: none -> 169 us  [on_device(): pl.pallas_call(kernel, out_shape=(jax.ShapeDtypeStruct((2, D, SERVED), bf...]
    all_to_all x2 -> x0, blocking collectives: 38 us -> none  [the longest x1 21.6 us: relayout(): lax.all_to_all(lax.all_to_all(stacked, 'tp', split_axis=1, concat_axis=2,...]
    dot_general x4 -> x0, matrix products: 32.3 us -> none  [the longest x2 24.5 us: half_step(): lax.dot_general(hidden, down_weight, (((1,), (1,)), ((), ())), preferred_...]
    unnamed x46 -> x15, local copies, waits for them, and re-layouts: 34.7 us -> 14.1 us
    all_to_all x2 -> x0, local copies, waits for them, and re-layouts: 18.6 us -> none  [the longest x1 9.73 us: relayout(): lax.all_to_all(lax.all_to_all(stacked, 'tp', split_axis=1, concat_axis=2,...]
    slice x7 -> x0, local copies, waits for them, and re-layouts: 13.8 us -> none  [the longest x2 7.52 us: on_device(): served_second[2]]
  transfers between devices with their start and end apart: 7 -> 0, of which waited for: 6 -> 0; matrix products, arithmetic and copies ran while one was open for 10% -> 0% of each run, Pallas kernels for 0% -> 0%
where the time goes in v1:
time: 194 us
  Pallas kernels  169 us (87%)
  local copies, waits for them, and re-layouts  21.1 us (11%)
  other arithmetic  2.9 us (1%)
    pallas_call x1, Pallas kernels, on_device(): pl.pallas_call(kernel, out_shape=(jax.ShapeDtypeStruct((2, D, SERVED), bf...  169 us
    unnamed x15, local copies, waits for them, and re-layouts  14.1 us
    squeeze x1, local copies, waits for them, and re-layouts, on_device(): served[t, :, m * PAD:m * PAD + BLK]  6.77 us

profile of v1, /device:TPU:2, one launch (start us, length us, event | category | flops | bytes accessed | tf_op | source)
XLA Modules:
  0.0 193.6 jit_solution(3997633331137664199)
XLA Ops:
  0.6 0.0 copy-start.3
  0.6 0.0 copy-start.1
  0.7 0.0 copy-start.2
  0.7 1.3 fusion.1
  2.0 0.1 concatenate.40
  2.1 0.0 copy-done.3
  2.1 0.0 copy-done.1
  2.1 0.0 copy-done.2
  2.1 0.8 fusion.3
  2.9 0.1 concatenate.44
  3.0 0.9 pad_maximum_fusion.packed
  3.9 168.9 %shard_map.144 = (bf16[2,2048,1152]{2,1,0:T(8,128)(2,1)}, bf16[96,2048]{1,0:T(8,128)(2,1)}) custom-call(bf16[2,64,2176]{2,1,0:T(8,128)(2,1)} %pad_maximum_fusion.packed, bf16[96,2048]{1,0:T(8,128)(2,1)} %prompt.1), custom_call_target="tpu_custom_call" | custom-call | tf_op jit(solution)/shard_map/pallas_call | solution.py:440
  172.8 6.8 %slice_bitcast_fusion = (bf16[2048,352]{1,0:T(8,128)(2,1)}, bf16[2048,352]{1,0:T(8,128)(2,1)}, bf16[2048,352]{1,0:T(8,128)(2,1)}, bf16[2048,352]{1,0:T(8,128)(2,...) fusion(bf16[2,2048,1152]{2,1,0:T(8,128)(2,1)} %get-tuple-element.9), kind=kLoop, calls=%fused_computation | loop fusion | bytes 17301504 | tf_op jit(solution)/shard_map/squeeze | solution.py:488
  179.5 2.5 %copy.21 = bf16[2048,352]{0,1:T(8,128)(2,1)} copy(bf16[2048,352]{1,0:T(8,128)(2,1)} %get-tuple-element.18) | data formatting | bytes 2883584
  182.1 2.5 %copy.20 = bf16[2048,352]{0,1:T(8,128)(2,1)} copy(bf16[2048,352]{1,0:T(8,128)(2,1)} %get-tuple-element.19) | data formatting | bytes 2883584
  184.6 2.5 %copy.19 = bf16[2048,352]{0,1:T(8,128)(2,1)} copy(bf16[2048,352]{1,0:T(8,128)(2,1)} %get-tuple-element.20) | data formatting | bytes 2883584
  187.2 2.5 %copy.18 = bf16[2048,352]{0,1:T(8,128)(2,1)} copy(bf16[2048,352]{1,0:T(8,128)(2,1)} %get-tuple-element.21) | data formatting | bytes 2883584
  189.7 1.6 copy.17
  191.3 0.0 copy-start
  191.3 1.6 copy.16
  192.8 0.0 copy-done
  192.8 0.7 copy.23
  (1 shorter events, 0.0 us)
Async XLA Ops:
  0.6 1.5 copy-start.3
  0.6 1.5 copy-start.1
  0.7 1.5 copy-start.2
  191.3 1.6 copy-start

commit v2 on v1

--- a/solution.py
+++ b/solution.py
@@ -15,18 +15,16 @@
 PIECE = 32
 COLS = 704
 BLK = 352
-PAD = 384
 PACK = 2176
 GU = 1408
 DN = 768
-SERVED = 3 * PAD
-NR = 17
-LANES = ((0, 768), (768, 640), (1408, 768))
+YP = (0, 896)
+ZQ = (896, 1280)
+GROUP = NY * ROWS
 CH = 512
 NCH = D // CH
 IN_SCALE = D ** (-0.5)
 OUT_SCALE = FF ** (-0.5)
-ROUNDS = 2 * NR + 10
 
 
 def kernel(
@@ -47,9 +45,16 @@
     rbuf,
     resid,
     stage,
+    picks,
     load_sem,
-    ring_recv,
-    ring_send,
+    yp_recv,
+    yp_send,
+    zq_recv,
+    zq_send,
+    zp_recv,
+    zp_send,
+    yq_recv,
+    yq_send,
     d2d_recv,
     d2d_send,
     srecv,
@@ -69,44 +74,34 @@
     z_lo, y = fs // NY, fs % NY
     z = gr * 4 + z_lo
     x, core = tp // 2, tp % 2
-    s = (y + z) % 4
 
     def dev(yy, zz, xx, cc):
         return (zz // 4, (zz % 4) * NY + yy, xx * 2 + cc)
 
     y_up, y_dn = (y + 1) % NY, (y + NY - 1) % NY
     z_up, z_dn = (z + 1) % NZ, (z + NZ - 1) % NZ
-    last = s // 3
-    first = (4 - s) // 4
-
-    def pick(flag, a, b):
-        return flag * a + (1 - flag) * b
-
-    nbr = (
-        (
-            dev(pick(last, y_up, y), pick(last, z, z_up), x, core),
-            dev(pick(first, y_dn, y), pick(first, z, z_dn), x, core),
-        ),
-        (
-            dev(pick(last, y, y_up), pick(last, z_up, z), x, core),
-            dev(pick(first, y, y_dn), pick(first, z_dn, z), x, core),
-        ),
-    )
+    along_y = (dev(y_up, z, x, core), dev(y_dn, z, x, core))
+    along_z = (dev(y, z_up, x, core), dev(y, z_dn, x, core))
     partner = dev(y, z, x, 1 - core)
     right = dev(y, z, (x + 1) % NX, core)
     left = dev(y, z, (x + NX - 1) % NX, core)
     x_r, x_l, x_far = (x + 1) % NX, (x + NX - 1) % NX, (x + 2) % NX
 
-    def piece_row(h, d, k):
-        if d == 0:
-            t = (k - s + 3) // 4
-            dy, dz = (t, k - t) if h == 0 else (k - t, t)
-            yy, zz = (y - dy + 32) % NY, (z - dz + 32) % NZ
+    near_y = (y, y_dn, y_up, (y + 2) % NY)
+
+    def from_z(d, k):
+        return (z + NZ - k) % NZ if d == 0 else (z + k) % NZ
+
+    def group_z(g):
+        return (z + NZ + (1 - 2 * (g % 2)) * ((g + 1) // 2)) % NZ
+
+    def piece(t, yy, zz, lanes, half=None):
+        row = (zz * NY + yy) * ROWS
+        if half is None:
+            rows = pl.ds(pl.multiple_of(row, ROWS), ROWS)
         else:
-            t = (s + k) // 4
-            dy, dz = (t, k - t) if h == 0 else (k - t, t)
-            yy, zz = (y + dy) % NY, (z + dz) % NZ
-        return pl.multiple_of((zz * NY + yy) * ROWS + h * PIECE, PIECE)
+            rows = pl.ds(pl.multiple_of(row + half * PIECE, PIECE), PIECE)
+        return wall.at[t, core, rows, pl.ds(*lanes)]
 
     def remote(src, dst, send, recv, device):
         return pltpu.make_async_remote_copy(
@@ -130,101 +125,128 @@
         load.start()
 
     barrier = pltpu.get_barrier_semaphore()
-    everyone = (
-        dev(y_up, z, x, core),
-        dev(y_dn, z, x, core),
-        dev(y, z_up, x, core),
-        dev(y, z_dn, x, core),
-        right,
-        left,
-        partner,
-    )
+    everyone = (*along_y, *along_z, right, left, partner)
     for device in everyone:
         pl.semaphore_signal(barrier, inc=1, device_id=device, device_id_type=pl.DeviceIdType.MESH)
     pl.semaphore_wait(barrier, len(everyone))
     for load in loads:
         load.wait()
 
-    def ring_round(R):
-        t = R // NR
-        r = R % NR
-        rows = {(h, d): pl.ds(piece_row(h, d, r), PIECE) for h in range(2) for d in range(2)}
-        for m, (lane, width) in enumerate(LANES):
-            for d in range(2):
-                end = 16 - d
-                blocks = [wall.at[t, core, rows[h, d], pl.ds(lane, width)] for h in range(2)]
-
-                @pl.when(jnp.logical_and(r >= 1, r <= end))
-                def _():
-                    for h in range(2):
-                        wait_for(blocks[h], ring_recv.at[R, h, d, m])
-
-                @pl.when(r < end)
-                def _():
-                    for h in range(2):
-                        remote(
-                            blocks[h],
-                            blocks[h],
-                            ring_send.at[t, h, d],
-                            ring_recv.at[R + 1, h, d, m],
-                            nbr[h][d],
-                        ).start()
-
-        for d in range(2):
-
-            @pl.when(jnp.logical_and(r >= d, r <= 16 - d))
-            def _():
-                for h in range(2):
-                    block = wall.at[t, core, rows[h, d]]
-                    remote(block, block, d2d_send.at[t], d2d_recv.at[t], partner).start()
+    def push(block, send, recv, device):
+        remote(block, block, send, recv, device).start()
+
+    def send_zp(t, k, i, origin_z):
+        half = k == 4
+        for d in range(2):
+            block = piece(t, near_y[i], origin_z[d], YP, d if half else None)
+            push(block, zp_send.at[t, d], zp_recv.at[t, d, k - 1, i], along_z[d])
+
+    def send_yq(t, g):
+        for d in range(2):
+            block = piece(t, y, group_z(g), ZQ)
+            push(block, yq_send.at[t, d], yq_recv.at[t, d, g, 0], along_y[d])
+
+    def begin(t):
+        for d in range(2):
+            push(piece(t, y, z, YP), yp_send.at[t, d], yp_recv.at[t, d, 0], along_y[d])
+            push(piece(t, y, z, ZQ), zq_send.at[t, d], zq_recv.at[t, d, 0], along_z[d])
+        send_zp(t, 1, 0, (z, z))
+        send_yq(t, 0)
+
+    def yp(t):
+        for d in range(2):
+            wait_for(piece(t, near_y[1 + d], z, YP), yp_recv.at[t, d, 0])
+            push(piece(t, near_y[1 + d], z, YP, d), yp_send.at[t, d], yp_recv.at[t, d, 1], along_y[d])
+        send_zp(t, 1, 1, (z, z))
+        send_zp(t, 1, 2, (z, z))
+
+    def yp_far(t):
+        for d in range(2):
+            wait_for(piece(t, near_y[3], z, YP, d), yp_recv.at[t, d, 1])
+        send_zp(t, 1, 3, (z, z))
+
+    def zq(t, k):
+        for d in range(2):
+            wait_for(piece(t, y, from_z(d, k), ZQ, d if k == 4 else None), zq_recv.at[t, d, k - 1])
+            if k < 4:
+                block = piece(t, y, from_z(d, k), ZQ, d if k == 3 else None)
+                push(block, zq_send.at[t, d], zq_recv.at[t, d, k], along_z[d])
+        send_yq(t, 2 * k - 1)
+        if k < 4:
+            send_yq(t, 2 * k)
+
+    def zp(t, k, i):
+        for d in range(2):
+            block = piece(t, near_y[i], from_z(d, k), YP, d if k == 4 else None)
+            wait_for(block, zp_recv.at[t, d, k - 1, i])
+        if k < 4:
+            send_zp(t, k + 1, i, (from_z(0, k), from_z(1, k)))
+
+    def yq(t, g):
+        for d in range(2):
+            wait_for(piece(t, near_y[1 + d], group_z(g), ZQ), yq_recv.at[t, d, g, 0])
+            block = piece(t, near_y[1 + d], group_z(g), ZQ, d)
+            push(block, yq_send.at[t, d], yq_recv.at[t, d, g, 1], along_y[d])
 
     serves = core == y // 2
     dist = ((x - z_lo + NX) % NX, (z_lo - x + NX) % NX)
     side = (right, left)
 
-    def cut(R):
-        t = R // NR
-        r = R % NR
-        for d in range(2):
-
-            @pl.when(jnp.logical_and(r >= d, r <= 16 - d))
-            def _():
-                for h in range(2):
-                    row = piece_row(h, d, r)
-                    for m, lane in enumerate((0, 640, 1408)):
-                        window = wall[t, core, pl.ds(row, PIECE), lane : lane + 768]
-                        window = window.astype(jnp.float32)
-                        start = (64 if m == 1 else 0) + BLK * (y % 2)
-                        block = pltpu.roll(window, (768 - start) % 768, 1)[:, :PAD]
-                        stage[R % 2, h, d, :, m * PAD : (m + 1) * PAD] = block.astype(jnp.bfloat16)
-                    pltpu.make_async_copy(
-                        stage.at[R % 2, h, d],
-                        served.at[t, pl.ds(row, PIECE)],
-                        srecv.at[R, h, d],
-                    ).start()
-
-    def pass_on(R):
+    def served_part(t, g, h):
+        lane = group_z(g) * GROUP + h * 128
+        return served.at[t, :, :, pl.ds(pl.multiple_of(lane, 128), 128)]
+
+    def make_picks():
+        for i in range(2):
+            unit = lax.broadcasted_iota(jnp.int32, (BLK, DN), 0)
+            lane = lax.broadcasted_iota(jnp.int32, (BLK, DN), 1)
+            wanted = unit + (BLK * (y % 2) + 64 * i)
+            picks[i] = jnp.where(lane == wanted, 1.0, 0.0).astype(jnp.bfloat16)
+
+    def cut(t, g):
+        rows = pl.ds(pl.multiple_of(group_z(g) * GROUP, GROUP), GROUP)
+        slot = g % 2
+        for m, lane in enumerate((0, 640, 1408)):
+            block = lax.dot_general(
+                picks[m % 2],
+                wall[t, core, rows, lane : lane + DN],
+                (((1,), (1,)), ((), ())),
+                preferred_element_type=jnp.float32,
+            ).astype(jnp.bfloat16)
+            for h in range(2):
+                stage[slot, h, m] = block[:, h * 128 : (h + 1) * 128]
         for h in range(2):
-            was = R - 2 * dist[h] - 1
-
-            @pl.when(jnp.logical_and(was >= 0, was < 2 * NR))
-            def _():
-                t = was // NR
-                r = was % NR
-                for d in range(2):
-
-                    @pl.when(jnp.logical_and(r >= d, r <= 16 - d))
+            pltpu.make_async_copy(
+                stage.at[slot, h], served_part(t, g, h), srecv.at[t * NZ + g, h]
+            ).start()
+
+    def pass_on(now):
+        @pl.when(serves)
+        def _():
+            for h in range(2):
+                was = now - 2 * dist[h] - 1
+
+                @pl.when(jnp.logical_and(was >= 0, was < 2 * NZ))
+                def _():
+                    block = served_part(was // NZ, was % NZ, h)
+                    wait_for(block, srecv.at[was, h])
+
+                    @pl.when(dist[h] < 3)
                     def _():
-                        block = served.at[t, pl.ds(piece_row(h, d, r), PIECE)]
-                        wait_for(block, srecv.at[was, h, d])
-
-                        @pl.when(dist[h] < 3)
-                        def _():
-                            remote(
-                                block, block, s_fwd_send.at[h], srecv.at[was, h, d], side[h]
-                            ).start()
-
-                        remote(block, block, s_d2d_send, s_d2d_recv, partner).start()
+                        push(block, s_fwd_send.at[h], srecv.at[was, h], side[h])
+
+                    push(block, s_d2d_send, s_d2d_recv, partner)
+
+    def whole(t, g):
+        for d in range(2):
+            wait_for(piece(t, near_y[3], group_z(g), ZQ, d), yq_recv.at[t, d, g, 1])
+        rows = pl.ds(pl.multiple_of(group_z(g) * GROUP, GROUP), GROUP)
+        push(wall.at[t, core, rows], d2d_send.at[t], d2d_recv.at[t], partner)
+        pass_on(t * NZ + g)
+
+        @pl.when(jnp.logical_and(serves, x == z_lo))
+        def _():
+            cut(t, g)
 
     def normed(value):
         square = jnp.mean(value * value, axis=-1, keepdims=True)
@@ -316,79 +338,143 @@
     resid[...] = start
     xa[0, x] = normed(start)
 
-    def one_round(R, carry):
-        @pl.when(R < 2 * NR)
-        def _():
-            ring_round(R)
-
-        @pl.when(R == 0)
-        def _():
-            send_tokens(0)
-
-        @pl.when(serves)
-        def _():
-            pass_on(R)
-
-            @pl.when(jnp.logical_and(x == z_lo, R < 2 * NR))
-            def _():
-                cut(R)
-
-        @pl.when(R == 3)
-        def _():
-            relay_tokens(0)
-
-        @pl.when(R == NR - 1)
-        def _():
-            await_tokens(0)
-
-        @pl.when(R == NR + 11)
-        def _():
-            relay_tokens(1)
-
-        @pl.when(R == 2 * NR - 1)
-        def _():
-            await_tokens(1)
-
-        t = (R - NR + NR) // NR - 1
-        q = R % NR
-
-        @pl.when(R >= NR)
-        def _():
-            @pl.when(q == 1)
-            def _():
-                wait_for(wall.at[t, 1 - core], d2d_recv.at[t])
-
-            @pl.when(q < 2)
-            def _():
-                hidden(t, (core + q) % 2)
-
-            @pl.when(jnp.logical_and(q >= 2, q < 2 + NCH))
-            def _():
-                down(t, q - 2)
-
-            @pl.when(jnp.logical_and(q >= 4, q < 4 + NCH))
-            def _():
-                combine(t, q - 4)
-
-        @pl.when(R == NR + 9)
-        def _():
-            middle = finish(0).astype(jnp.float32)
-            resid[...] = middle
-            xa[1, x] = normed(middle)
-            send_tokens(1)
-
-        @pl.when(R == 2 * NR + 9)
-        def _():
-            result[...] = finish(1)
-
-        return carry
-
-    lax.fori_loop(0, ROUNDS, one_round, 0)
+    begin(0)
+    send_tokens(0)
+    make_picks()
+
+    def compute(t, stage_of):
+        if stage_of == 0:
+            hidden(t, core)
+        elif stage_of == 1:
+            wait_for(wall.at[t, 1 - core], d2d_recv.at[t])
+            hidden(t, 1 - core)
+
+    def to_second():
+        middle = finish(0).astype(jnp.float32)
+        resid[...] = middle
+        xa[1, x] = normed(middle)
+        send_tokens(1)
+
+    yp(0)
+    zq(0, 1)
+    zp(0, 1, 0)
+    yq(0, 0)
+    yp_far(0)
+    zp(0, 1, 1)
+    zp(0, 1, 2)
+    zp(0, 1, 3)
+    relay_tokens(0)
+    zq(0, 2)
+    whole(0, 0)
+    zp(0, 2, 0)
+    yq(0, 1)
+    yq(0, 2)
+    zp(0, 2, 1)
+    zp(0, 2, 2)
+    zp(0, 2, 3)
+    zq(0, 3)
+    whole(0, 1)
+    whole(0, 2)
+    zp(0, 3, 0)
+    yq(0, 3)
+    yq(0, 4)
+    zp(0, 3, 1)
+    zp(0, 3, 2)
+    zp(0, 3, 3)
+    zq(0, 4)
+    begin(1)
+    whole(0, 3)
+    whole(0, 4)
+    zp(0, 4, 0)
+    yq(0, 5)
+    yq(0, 6)
+    zp(0, 4, 1)
+    zp(0, 4, 2)
+    zp(0, 4, 3)
+    yq(0, 7)
+    yp(1)
+    zq(1, 1)
+    whole(0, 5)
+    whole(0, 6)
+    zp(1, 1, 0)
+    whole(0, 7)
+    await_tokens(0)
+    yq(1, 0)
+    yp_far(1)
+    compute(0, 0)
+    zp(1, 1, 1)
+    zp(1, 1, 2)
+    zp(1, 1, 3)
+    zq(1, 2)
+    compute(0, 1)
+    whole(1, 0)
+    zp(1, 2, 0)
+    down(0, 0)
+    yq(1, 1)
+    down(0, 1)
+    yq(1, 2)
+    zp(1, 2, 1)
+    down(0, 2)
+    combine(0, 0)
+    zp(1, 2, 2)
+    down(0, 3)
+    combine(0, 1)
+    zp(1, 2, 3)
+    zq(1, 3)
+    combine(0, 2)
+    whole(1, 1)
+    combine(0, 3)
+    whole(1, 2)
+    zp(1, 3, 0)
+    yq(1, 3)
+    yq(1, 4)
+    zp(1, 3, 1)
+    zp(1, 3, 2)
+    zp(1, 3, 3)
+    to_second()
+    zq(1, 4)
+    whole(1, 3)
+    whole(1, 4)
+    zp(1, 4, 0)
+    relay_tokens(1)
+    yq(1, 5)
+    yq(1, 6)
+    zp(1, 4, 1)
+    zp(1, 4, 2)
+    zp(1, 4, 3)
+    whole(1, 5)
+    whole(1, 6)
+    yq(1, 7)
+    whole(1, 7)
+    await_tokens(1)
+    pass_on(16)
+    compute(1, 0)
+    pass_on(17)
+    compute(1, 1)
+    down(1, 0)
+    pass_on(18)
+    down(1, 1)
+    down(1, 2)
+    combine(1, 0)
+    pass_on(19)
+    down(1, 3)
+    combine(1, 1)
+    pass_on(20)
+    combine(1, 2)
+    pass_on(21)
+    combine(1, 3)
+    pass_on(22)
+    result[...] = finish(1)
+
+    def some(rows, lanes):
+        return wall.at[0, 0, pl.ds(0, rows), pl.ds(*lanes)]
 
     for t in range(2):
-        for h in range(2):
-            wait_for(wall.at[t, 0, pl.ds(0, 16 * PIECE)], ring_send.at[t, h, 0])
-            wait_for(wall.at[t, 0, pl.ds(0, 15 * PIECE)], ring_send.at[t, h, 1])
+        for d in range(2):
+            wait_for(some(96, YP), yp_send.at[t, d])
+            wait_for(some(NZ * 96, ZQ), yq_send.at[t, d])
+            wait_for(some(224, ZQ), zq_send.at[t, d])
+            wait_for(some(NY * 224, YP), zp_send.at[t, d])
         wait_for(wall.at[t, core], d2d_send.at[t])
         for i in range(2):
             for b in range(3):
@@ -440,7 +526,7 @@
     served, result = pl.pallas_call(
         kernel,
         out_shape=(
-            jax.ShapeDtypeStruct((2, D, SERVED), bf16),
+            jax.ShapeDtypeStruct((2, 3, BLK, D), bf16),
             jax.ShapeDtypeStruct((TOK, D), bf16),
         ),
         in_specs=[
@@ -464,13 +550,20 @@
             pltpu.VMEM((2, 2, HALF, D), bf16),
             pltpu.VMEM((2, 2, TOK, D), bf16),
             pltpu.VMEM((TOK, D), f32),
-            pltpu.VMEM((2, 2, 2, PIECE, SERVED), bf16),
+            pltpu.VMEM((2, 2, 3, BLK, 128), bf16),
+            pltpu.VMEM((2, BLK, DN), bf16),
             dma((2,)),
-            dma((2 * NR, 2, 2, 3)),
             dma((2, 2, 2)),
+            dma((2, 2)),
+            dma((2, 2, 4)),
+            dma((2, 2)),
+            dma((2, 2, 4, NY)),
+            dma((2, 2)),
+            dma((2, 2, NZ, 2)),
+            dma((2, 2)),
             dma((2,)),
             dma((2,)),
-            dma((2 * NR, 2, 2)),
+            dma((2 * NZ, 2)),
             dma((2,)),
             dma,
             dma,
@@ -485,7 +578,7 @@
             collective_id=0, has_side_effects=True, vmem_limit_bytes=66 * 1024 * 1000
         ),
     )(packed, prompt)
-    blocks = [served[t, :, m * PAD : m * PAD + BLK] for t in range(2) for m in range(3)]
+    blocks = [served[t, m].T for t in range(2) for m in range(3)]
     return (*blocks, result)
 
 

time: 194 us -> 175 us (0.902)
  local copies, waits for them, and re-layouts: 21.1 us -> 7.26 us
  Pallas kernels: 169 us -> 164 us
    unnamed x15 -> x11, local copies, waits for them, and re-layouts: 14.1 us -> 0.77 us
    squeeze x1 -> x0, local copies, waits for them, and re-layouts: 6.77 us -> none  [on_device(): served[t, :, m * PAD:m * PAD + BLK]]
    transpose x0 -> x1, local copies, waits for them, and re-layouts: none -> 6.2 us  [on_device(): blocks = [served[t, m].T for t in range(2) for m in range(3)]]
    pallas_call x1, Pallas kernels: 169 us -> 164 us  [on_device(): pl.pallas_call(kernel, out_shape=(jax.ShapeDtypeStruct((2, 3, BLK, D), bf...]
where the time goes in v2:
time: 175 us
  Pallas kernels  164 us (94%)
  local copies, waits for them, and re-layouts  7.26 us (4%)
  other arithmetic  2.24 us (1%)
    pallas_call x1, Pallas kernels, on_device(): pl.pallas_call(kernel, out_shape=(jax.ShapeDtypeStruct((2, 3, BLK, D), bf...  164 us
    transpose x1, local copies, waits for them, and re-layouts, on_device(): blocks = [served[t, m].T for t in range(2) for m in range(3)]  6.2 us

profile of v2, /device:TPU:2, one launch (start us, length us, event | category | flops | bytes accessed | tf_op | source)
XLA Modules:
  0.0 174.6 jit_solution(14426770548075904642)
XLA Ops:
  0.6 0.0 copy-start.3
  0.6 0.0 copy-start.1
  0.7 0.0 copy-start.2
  0.7 0.0 copy-start.4
  0.7 1.3 fusion.1
  2.0 0.1 concatenate.40
  2.1 0.0 copy-done.3
  2.1 0.0 copy-done.1
  2.1 0.0 copy-done.2
  2.2 0.0 copy-done.4
  2.2 0.1 fusion.3
  2.3 0.1 concatenate.44
  2.4 0.9 pad_maximum_fusion.packed
  3.3 164.4 %shard_map.144 = (bf16[2,3,352,2048]{3,2,1,0:T(8,128)(2,1)}, bf16[96,2048]{1,0:T(8,128)(2,1)}) custom-call(bf16[2,64,2176]{2,1,0:T(8,128)(2,1)} %pad_maximum_fusion.packed, bf16[96,2048]{1,0:T(8,128)(2,1)} %prompt.1), custom_call_target="tpu_custom_call" | custom-call | tf_op jit(solution)/shard_map/pallas_call | solution.py:526
  167.6 0.0 copy-start
  167.6 6.2 %slice_bitcast_fusion = (bf16[2048,352]{0,1:T(8,128)(2,1)}, bf16[2048,352]{0,1:T(8,128)(2,1)}, bf16[2048,352]{0,1:T(8,128)(2,1)}, bf16[2048,352]{0,1:T(8,128)(2,...) fusion(bf16[2,3,352,2048]{3,2,1,0:T(8,128)(2,1)} %get-tuple-element.9), kind=kLoop, calls=%fused_computation | loop fusion | bytes 17301504 | tf_op jit(solution)/shard_map/transpose | solution.py:581
  173.8 0.0 copy-done
  173.8 0.7 copy.17
  (1 shorter events, 0.0 us)
Async XLA Ops:
  0.6 1.5 copy-start.3
  0.6 1.5 copy-start.1
  0.7 1.5 copy-start.2
  0.7 1.5 copy-start.4
  167.6 6.2 %copy-start = (bf16[96,2048]{1,0:T(8,128)(2,1)S(1)}, bf16[96,2048]{1,0:T(8,128)(2,1)}, u32[]{:S(2)}) copy-start(bf16[96,2048]{1,0:T(8,128)(2,1)} %get-tuple-element.36) | copy-start | bytes 1179652

commit v3 on v2

--- a/solution.py
+++ b/solution.py
@@ -18,13 +18,73 @@
 PACK = 2176
 GU = 1408
 DN = 768
-YP = (0, 896)
-ZQ = (896, 1280)
+YP = ((0, 640), (1408, 256))
+ZQ = ((640, 768), (1664, 512))
+ALL = ((0, 1408), (1408, 768))
+STREAMS = 4
 GROUP = NY * ROWS
-CH = 512
-NCH = D // CH
+CH = GROUP
+NCH = NZ
 IN_SCALE = D ** (-0.5)
 OUT_SCALE = FF ** (-0.5)
+
+
+STARTS = (0.0, 18.0, 46.0, 66.0)
+PACES = (10.5, 9.5, 11.0, 9.5)
+
+
+def plan():
+    steps = []
+
+    def at(time, name, *args):
+        steps.append((time, name, args))
+
+    at(STARTS[0] - 0.3, "send_tokens", 0)
+    at(STARTS[0] - 0.2, "make_picks")
+    at(9.0, "relay_tokens", 0)
+    ready = {}
+    for t, (b, pace) in enumerate(zip(STARTS, PACES)):
+        at(b - 0.5, "begin", t)
+        at(b + 5.5, "yp", t)
+        at(b + 9.8, "yp_far", t)
+        at(b + 7.0 + 0.3 * pace, "yq", t, 0)
+        for k in range(1, 5):
+            base = b + 7.0 + (k - 1) * pace
+            at(base, "zq", t, k)
+            for i in range(4):
+                at(base + pace * (0.2 + i * 0.18) + (0.1 if k == 1 else 0.0), "zp", t, k, i)
+            if k < 4:
+                at(base + pace * 0.84, "yq", t, 2 * k - 1)
+                at(base + pace * 0.92, "yq", t, 2 * k)
+            else:
+                at(base + pace * 0.76, "yq", t, 7)
+        done = [b + 7.0 + pace]
+        for k in range(1, 4):
+            done += [b + 7.0 + pace * (k + 0.5) + 0.8 * w for w in range(2)]
+        done.append(b + 7.0 + 4 * pace)
+        for g in range(NZ):
+            at(done[g], "whole", t, g)
+            ready[t, g] = done[g]
+            for d in range(4):
+                hops = 1 if t == STREAMS - 1 and d == 3 else d
+                lag = 1.5 + hops * (6.5 if t % 2 == 0 else 5.5)
+                at(done[g] + lag, "pass_on", t * NZ + g, d)
+    for t in range(2):
+        go = ready[2 * t, 7] + 0.3
+        at(go, "await_tokens", t)
+        at(go + 0.1, "compute", t, 0)
+        at(go + 4.5, "compute", t, 1)
+        then = go + 8.0
+        for g in range(NZ):
+            then = max(then + 0.9, ready[2 * t + 1, g] + 2.5)
+            at(then, "down", t, g)
+            at(then + 5.5, "combine", t, g)
+        if t == 0:
+            at(then + 14.0, "to_second")
+            at(then + 22.0, "relay_tokens", 1)
+        else:
+            at(then + 12.0, "last_step")
+    return sorted(steps, key=lambda step: step[0])
 
 
 def kernel(
@@ -59,6 +119,7 @@
     d2d_send,
     srecv,
     s_fwd_send,
+    s_last_send,
     s_d2d_send,
     s_d2d_recv,
     ag_recv,
@@ -96,12 +157,13 @@
         return (z + NZ + (1 - 2 * (g % 2)) * ((g + 1) // 2)) % NZ
 
     def piece(t, yy, zz, lanes, half=None):
+        lanes = lanes[t % 2]
         row = (zz * NY + yy) * ROWS
         if half is None:
             rows = pl.ds(pl.multiple_of(row, ROWS), ROWS)
         else:
             rows = pl.ds(pl.multiple_of(row + half * PIECE, PIECE), PIECE)
-        return wall.at[t, core, rows, pl.ds(*lanes)]
+        return wall.at[t // 2, core, rows, pl.ds(*lanes)]
 
     def remote(src, dst, send, recv, device):
         return pltpu.make_async_remote_copy(
@@ -192,9 +254,10 @@
     dist = ((x - z_lo + NX) % NX, (z_lo - x + NX) % NX)
     side = (right, left)
 
-    def served_part(t, g, h):
-        lane = group_z(g) * GROUP + h * 128
-        return served.at[t, :, :, pl.ds(pl.multiple_of(lane, 128), 128)]
+    def served_part(t, kind, g, h):
+        lane = pl.multiple_of(group_z(g) * GROUP + h * 128, 128)
+        which = pl.ds(2, 1) if kind else pl.ds(0, 2)
+        return served.at[t, which, :, pl.ds(lane, 128)]
 
     def make_picks():
         for i in range(2):
@@ -206,43 +269,50 @@
     def cut(t, g):
         rows = pl.ds(pl.multiple_of(group_z(g) * GROUP, GROUP), GROUP)
         slot = g % 2
-        for m, lane in enumerate((0, 640, 1408)):
+        kind = t % 2
+        for m, lane in ((2, GU),) if kind else ((0, 0), (1, 640)):
             block = lax.dot_general(
                 picks[m % 2],
-                wall[t, core, rows, lane : lane + DN],
+                wall[t // 2, core, rows, lane : lane + DN],
                 (((1,), (1,)), ((), ())),
                 preferred_element_type=jnp.float32,
             ).astype(jnp.bfloat16)
             for h in range(2):
                 stage[slot, h, m] = block[:, h * 128 : (h + 1) * 128]
         for h in range(2):
+            src = stage.at[slot, h, pl.ds(2, 1) if kind else pl.ds(0, 2)]
             pltpu.make_async_copy(
-                stage.at[slot, h], served_part(t, g, h), srecv.at[t * NZ + g, h]
+                src, served_part(t // 2, kind, g, h), srecv.at[t * NZ + g, h]
             ).start()
 
-    def pass_on(now):
+    def pass_on(e, d):
+        t, g = e // NZ, e % NZ
+
         @pl.when(serves)
         def _():
             for h in range(2):
-                was = now - 2 * dist[h] - 1
-
-                @pl.when(jnp.logical_and(was >= 0, was < 2 * NZ))
+
+                @pl.when(dist[h] == d)
                 def _():
-                    block = served_part(was // NZ, was % NZ, h)
-                    wait_for(block, srecv.at[was, h])
-
-                    @pl.when(dist[h] < 3)
-                    def _():
-                        push(block, s_fwd_send.at[h], srecv.at[was, h], side[h])
-
+                    block = served_part(t // 2, t % 2, g, h)
+                    wait_for(block, srecv.at[e, h])
+                    if t < STREAMS - 1:
+                        if d < 3:
+                            push(block, s_fwd_send.at[t // 2, h], srecv.at[e, h], side[h])
+                    elif d == 0:
+                        for device in side:
+                            push(block, s_last_send.at[h], srecv.at[e, h], device)
+                    elif d == 1:
+                        push(block, s_last_send.at[h], srecv.at[e, h], side[h])
                     push(block, s_d2d_send, s_d2d_recv, partner)
 
     def whole(t, g):
         for d in range(2):
             wait_for(piece(t, near_y[3], group_z(g), ZQ, d), yq_recv.at[t, d, g, 1])
         rows = pl.ds(pl.multiple_of(group_z(g) * GROUP, GROUP), GROUP)
-        push(wall.at[t, core, rows], d2d_send.at[t], d2d_recv.at[t], partner)
-        pass_on(t * NZ + g)
+        block = wall.at[t // 2, core, rows, pl.ds(*ALL[t % 2])]
+        landed = d2d_recv.at[t // 2, g if t % 2 else NZ]
+        push(block, d2d_send.at[t], landed, partner)
 
         @pl.when(jnp.logical_and(serves, x == z_lo))
         def _():
@@ -286,8 +356,12 @@
 
         lax.fori_loop(0, NX * TOK // HALF, rows_of, 0)
 
+    def columns(g):
+        return pl.ds(pl.multiple_of(group_z(g) * CH, CH), CH)
+
     def down(t, j):
-        drows = pl.ds(pl.multiple_of(j * CH, CH), CH)
+        drows = columns(j)
+        wait_for(wall.at[t, 1 - core, drows, pl.ds(*ALL[1])], d2d_recv.at[t, j])
         total = None
         for c in range(2):
             term = lax.dot_general(
@@ -312,7 +386,7 @@
             ).start()
 
     def combine(t, j):
-        drows = pl.ds(pl.multiple_of(j * CH, CH), CH)
+        drows = columns(j)
         for i, device in enumerate((right, left)):
             wait_for(cbuf.at[t, i, :, drows], c_recv.at[t, i, j])
             comb[t, i, halves[i], drows] = (
@@ -330,23 +404,19 @@
     def finish(t):
         for j in range(NCH):
             for i in range(2):
-                wait_for(rbuf.at[t, i, :, pl.ds(j * CH, CH)], r_recv.at[t, i, j])
+                wait_for(rbuf.at[t, i, :, columns(j)], r_recv.at[t, i, j])
         branch = own[...] + rbuf[t, 0].astype(jnp.float32) + rbuf[t, 1].astype(jnp.float32)
         return (resid[...] + 0.5 * branch).astype(jnp.bfloat16)
 
     start = prompt[...].astype(jnp.float32)
     resid[...] = start
     xa[0, x] = normed(start)
-
-    begin(0)
-    send_tokens(0)
-    make_picks()
 
     def compute(t, stage_of):
         if stage_of == 0:
             hidden(t, core)
         elif stage_of == 1:
-            wait_for(wall.at[t, 1 - core], d2d_recv.at[t])
+            wait_for(wall.at[t, 1 - core, :, pl.ds(*ALL[0])], d2d_recv.at[t, NZ])
             hidden(t, 1 - core)
 
     def to_second():
@@ -355,127 +425,43 @@
         xa[1, x] = normed(middle)
         send_tokens(1)
 
-    yp(0)
-    zq(0, 1)
-    zp(0, 1, 0)
-    yq(0, 0)
-    yp_far(0)
-    zp(0, 1, 1)
-    zp(0, 1, 2)
-    zp(0, 1, 3)
-    relay_tokens(0)
-    zq(0, 2)
-    whole(0, 0)
-    zp(0, 2, 0)
-    yq(0, 1)
-    yq(0, 2)
-    zp(0, 2, 1)
-    zp(0, 2, 2)
-    zp(0, 2, 3)
-    zq(0, 3)
-    whole(0, 1)
-    whole(0, 2)
-    zp(0, 3, 0)
-    yq(0, 3)
-    yq(0, 4)
-    zp(0, 3, 1)
-    zp(0, 3, 2)
-    zp(0, 3, 3)
-    zq(0, 4)
-    begin(1)
-    whole(0, 3)
-    whole(0, 4)
-    zp(0, 4, 0)
-    yq(0, 5)
-    yq(0, 6)
-    zp(0, 4, 1)
-    zp(0, 4, 2)
-    zp(0, 4, 3)
-    yq(0, 7)
-    yp(1)
-    zq(1, 1)
-    whole(0, 5)
-    whole(0, 6)
-    zp(1, 1, 0)
-    whole(0, 7)
-    await_tokens(0)
-    yq(1, 0)
-    yp_far(1)
-    compute(0, 0)
-    zp(1, 1, 1)
-    zp(1, 1, 2)
-    zp(1, 1, 3)
-    zq(1, 2)
-    compute(0, 1)
-    whole(1, 0)
-    zp(1, 2, 0)
-    down(0, 0)
-    yq(1, 1)
-    down(0, 1)
-    yq(1, 2)
-    zp(1, 2, 1)
-    down(0, 2)
-    combine(0, 0)
-    zp(1, 2, 2)
-    down(0, 3)
-    combine(0, 1)
-    zp(1, 2, 3)
-    zq(1, 3)
-    combine(0, 2)
-    whole(1, 1)
-    combine(0, 3)
-    whole(1, 2)
-    zp(1, 3, 0)
-    yq(1, 3)
-    yq(1, 4)
-    zp(1, 3, 1)
-    zp(1, 3, 2)
-    zp(1, 3, 3)
-    to_second()
-    zq(1, 4)
-    whole(1, 3)
-    whole(1, 4)
-    zp(1, 4, 0)
-    relay_tokens(1)
-    yq(1, 5)
-    yq(1, 6)
-    zp(1, 4, 1)
-    zp(1, 4, 2)
-    zp(1, 4, 3)
-    whole(1, 5)
-    whole(1, 6)
-    yq(1, 7)
-    whole(1, 7)
-    await_tokens(1)
-    pass_on(16)
-    compute(1, 0)
-    pass_on(17)
-    compute(1, 1)
-    down(1, 0)
-    pass_on(18)
-    down(1, 1)
-    down(1, 2)
-    combine(1, 0)
-    pass_on(19)
-    down(1, 3)
-    combine(1, 1)
-    pass_on(20)
-    combine(1, 2)
-    pass_on(21)
-    combine(1, 3)
-    pass_on(22)
-    result[...] = finish(1)
+    def last_step():
+        result[...] = finish(1)
+
+    steps = dict(
+        begin=begin,
+        yp=yp,
+        yp_far=yp_far,
+        zq=zq,
+        zp=zp,
+        yq=yq,
+        whole=whole,
+        pass_on=pass_on,
+        send_tokens=send_tokens,
+        relay_tokens=relay_tokens,
+        await_tokens=await_tokens,
+        make_picks=make_picks,
+        compute=compute,
+        down=down,
+        combine=combine,
+        to_second=to_second,
+        last_step=last_step,
+    )
+    for _, name, args in plan():
+        steps[name](*args)
 
     def some(rows, lanes):
         return wall.at[0, 0, pl.ds(0, rows), pl.ds(*lanes)]
 
+    for t in range(STREAMS):
+        p_lanes, q_lanes = YP[t % 2], ZQ[t % 2]
+        for d in range(2):
+            wait_for(some(96, p_lanes), yp_send.at[t, d])
+            wait_for(some(NZ * 96, q_lanes), yq_send.at[t, d])
+            wait_for(some(224, q_lanes), zq_send.at[t, d])
+            wait_for(some(NY * 224, p_lanes), zp_send.at[t, d])
+        wait_for(some(D, ALL[t % 2]), d2d_send.at[t])
     for t in range(2):
-        for d in range(2):
-            wait_for(some(96, YP), yp_send.at[t, d])
-            wait_for(some(NZ * 96, ZQ), yq_send.at[t, d])
-            wait_for(some(224, ZQ), zq_send.at[t, d])
-            wait_for(some(NY * 224, YP), zp_send.at[t, d])
-        wait_for(wall.at[t, core], d2d_send.at[t])
         for i in range(2):
             for b in range(3):
                 wait_for(xa.at[t, x, halves[0]], ag_send.at[t, i, b])
@@ -488,9 +474,18 @@
     def _():
         for h in range(2):
 
+            half = pl.ds(0, D // 2)
+
             @pl.when(dist[h] < 3)
             def _():
-                wait_for(served.at[0], s_fwd_send.at[h])
+                wait_for(served.at[0, :, :, half], s_fwd_send.at[0, h])
+                wait_for(served.at[0, pl.ds(0, 2), :, half], s_fwd_send.at[1, h])
+
+            for d, sends in ((0, 2), (1, 1)):
+
+                @pl.when(dist[h] == d)
+                def _():
+                    wait_for(served.at[0, pl.ds(0, sends), :, half], s_last_send.at[h])
 
         wait_for(served, s_d2d_send)
 
@@ -553,17 +548,18 @@
             pltpu.VMEM((2, 2, 3, BLK, 128), bf16),
             pltpu.VMEM((2, BLK, DN), bf16),
             dma((2,)),
-            dma((2, 2, 2)),
+            dma((STREAMS, 2, 2)),
+            dma((STREAMS, 2)),
+            dma((STREAMS, 2, 4)),
+            dma((STREAMS, 2)),
+            dma((STREAMS, 2, 4, NY)),
+            dma((STREAMS, 2)),
+            dma((STREAMS, 2, NZ, 2)),
+            dma((STREAMS, 2)),
+            dma((2, NZ + 1)),
+            dma((STREAMS,)),
+            dma((STREAMS * NZ, 2)),
             dma((2, 2)),
-            dma((2, 2, 4)),
-            dma((2, 2)),
-            dma((2, 2, 4, NY)),
-            dma((2, 2)),
-            dma((2, 2, NZ, 2)),
-            dma((2, 2)),
-            dma((2,)),
-            dma((2,)),
-            dma((2 * NZ, 2)),
             dma((2,)),
             dma,
             dma,

time: 175 us -> 171 us (0.977); the launches traced: 175 us -> 169 us
  Pallas kernels: 164 us -> 159 us
    pallas_call x1, Pallas kernels: 164 us -> 159 us  [on_device(): pl.pallas_call(kernel, out_shape=(jax.ShapeDtypeStruct((2, 3, BLK, D), bf...]
where the time goes in v3:
time: 171 us; the launch traced here: 169 us
  Pallas kernels  159 us (93%)
  local copies, waits for them, and re-layouts  7.26 us (4%)
  other arithmetic  2.24 us (1%)
    pallas_call x1, Pallas kernels, on_device(): pl.pallas_call(kernel, out_shape=(jax.ShapeDtypeStruct((2, 3, BLK, D), bf...  159 us
    transpose x1, local copies, waits for them, and re-layouts, on_device(): blocks = [served[t, m].T for t in range(2) for m in range(3)]  6.2 us

profile of v3, /device:TPU:2, one launch (start us, length us, event | category | flops | bytes accessed | tf_op | source)
XLA Modules:
  0.0 168.8 jit_solution(9735439927260618914)
XLA Ops:
  0.6 0.0 copy-start.3
  0.6 0.0 copy-start.1
  0.7 0.0 copy-start.2
  0.7 0.0 copy-start.4
  0.7 1.3 fusion.1
  2.0 0.1 concatenate.40
  2.1 0.0 copy-done.3
  2.1 0.0 copy-done.1
  2.1 0.0 copy-done.2
  2.2 0.0 copy-done.4
  2.2 0.1 fusion.3
  2.3 0.1 concatenate.44
  2.4 0.9 pad_maximum_fusion.packed
  3.3 158.6 %shard_map.144 = (bf16[2,3,352,2048]{3,2,1,0:T(8,128)(2,1)}, bf16[96,2048]{1,0:T(8,128)(2,1)}) custom-call(bf16[2,64,2176]{2,1,0:T(8,128)(2,1)} %pad_maximum_fusion.packed, bf16[96,2048]{1,0:T(8,128)(2,1)} %prompt.1), custom_call_target="tpu_custom_call" | custom-call | tf_op jit(solution)/shard_map/pallas_call | solution.py:521
  161.9 0.0 copy-start
  161.9 6.2 %slice_bitcast_fusion = (bf16[2048,352]{0,1:T(8,128)(2,1)}, bf16[2048,352]{0,1:T(8,128)(2,1)}, bf16[2048,352]{0,1:T(8,128)(2,1)}, bf16[2048,352]{0,1:T(8,128)(2,...) fusion(bf16[2,3,352,2048]{3,2,1,0:T(8,128)(2,1)} %get-tuple-element.9), kind=kLoop, calls=%fused_computation | loop fusion | bytes 17301504 | tf_op jit(solution)/shard_map/transpose | solution.py:577
  168.1 0.0 copy-done
  168.1 0.7 copy.17
  (1 shorter events, 0.0 us)
Async XLA Ops:
  0.6 1.5 copy-start.3
  0.6 1.5 copy-start.1
  0.7 1.5 copy-start.2
  0.7 1.5 copy-start.4
  161.9 6.2 %copy-start = (bf16[96,2048]{1,0:T(8,128)(2,1)S(1)}, bf16[96,2048]{1,0:T(8,128)(2,1)}, u32[]{:S(2)}) copy-start(bf16[96,2048]{1,0:T(8,128)(2,1)} %get-tuple-element.36) | copy-start | bytes 1179652

commit v4 on v3

--- a/solution.py
+++ b/solution.py
@@ -408,9 +408,6 @@
         branch = own[...] + rbuf[t, 0].astype(jnp.float32) + rbuf[t, 1].astype(jnp.float32)
         return (resid[...] + 0.5 * branch).astype(jnp.bfloat16)
 
-    start = prompt[...].astype(jnp.float32)
-    resid[...] = start
-    xa[0, x] = normed(start)
 
     def compute(t, stage_of):
         if stage_of == 0:
@@ -424,6 +421,12 @@
         resid[...] = middle
         xa[1, x] = normed(middle)
         send_tokens(1)
+
+    def first_tokens(p):
+        start = prompt[...].astype(jnp.float32)
+        resid[...] = start
+        xa[p, x] = normed(start)
+        send_tokens(p)
 
     def last_step():
         result[...] = finish(1)
@@ -437,7 +440,7 @@
         yq=yq,
         whole=whole,
         pass_on=pass_on,
-        send_tokens=send_tokens,
+        send_tokens=first_tokens,
         relay_tokens=relay_tokens,
         await_tokens=await_tokens,
         make_picks=make_picks,

time: 171 us -> 171 us (level)
  no operation moved by 1% of the time
where the time goes in v4:
time: 171 us; the launch traced here: 169 us
  Pallas kernels  159 us (93%)
  local copies, waits for them, and re-layouts  7.26 us (4%)
  other arithmetic  2.24 us (1%)
    pallas_call x1, Pallas kernels, on_device(): pl.pallas_call(kernel, out_shape=(jax.ShapeDtypeStruct((2, 3, BLK, D), bf...  159 us
    transpose x1, local copies, waits for them, and re-layouts, on_device(): blocks = [served[t, m].T for t in range(2) for m in range(3)]  6.2 us

profile of v4, /device:TPU:2, one launch (start us, length us, event | category | flops | bytes accessed | tf_op | source)
XLA Modules:
  0.0 168.9 jit_solution(13102079010429355993)
XLA Ops:
  0.6 0.0 copy-start.3
  0.6 0.0 copy-start.1
  0.7 0.0 copy-start.2
  0.7 0.0 copy-start.4
  0.7 1.3 fusion.1
  2.0 0.1 concatenate.40
  2.1 0.0 copy-done.3
  2.1 0.0 copy-done.1
  2.1 0.0 copy-done.2
  2.2 0.0 copy-done.4
  2.2 0.1 fusion.3
  2.3 0.1 concatenate.44
  2.4 0.9 pad_maximum_fusion.packed
  3.3 158.6 %shard_map.144 = (bf16[2,3,352,2048]{3,2,1,0:T(8,128)(2,1)}, bf16[96,2048]{1,0:T(8,128)(2,1)}) custom-call(bf16[2,64,2176]{2,1,0:T(8,128)(2,1)} %pad_maximum_fusion.packed, bf16[96,2048]{1,0:T(8,128)(2,1)} %prompt.1), custom_call_target="tpu_custom_call" | custom-call | tf_op jit(solution)/shard_map/pallas_call | solution.py:524
  161.9 0.0 copy-start
  161.9 6.2 %slice_bitcast_fusion = (bf16[2048,352]{0,1:T(8,128)(2,1)}, bf16[2048,352]{0,1:T(8,128)(2,1)}, bf16[2048,352]{0,1:T(8,128)(2,1)}, bf16[2048,352]{0,1:T(8,128)(2,...) fusion(bf16[2,3,352,2048]{3,2,1,0:T(8,128)(2,1)} %get-tuple-element.9), kind=kLoop, calls=%fused_computation | loop fusion | bytes 17301504 | tf_op jit(solution)/shard_map/transpose | solution.py:580
  168.1 0.0 copy-done
  168.1 0.7 copy.17
  (1 shorter events, 0.0 us)
Async XLA Ops:
  0.6 1.5 copy-start.3
  0.6 1.5 copy-start.1
  0.7 1.5 copy-start.2
  0.7 1.5 copy-start.4
  161.9 6.2 %copy-start = (bf16[96,2048]{1,0:T(8,128)(2,1)S(1)}, bf16[96,2048]{1,0:T(8,128)(2,1)}, u32[]{:S(2)}) copy-start(bf16[96,2048]{1,0:T(8,128)(2,1)} %get-tuple-element.36) | copy-start | bytes 1179652
